TPU v7x, 256 devices: a whole 4x4x8 slice. The times are simulated.
256 devices in a mesh: rep: 2 (over z_hi), fs: 16 (over z_lo, y), tp: 8 (over x, core).
Axes of the slice: x: 4, y: 4, z: 8 (z_hi: 2, z_lo: 4; z = z_hi * 4 + z_lo), core: 2. Of those that a mesh axis runs over, the one named last changes fastest.
Arguments:
- stream: bfloat16 [32, 1024, 2048], P(('rep', 'fs'), None, 'tp'), may hold values from -6 to 6
- norm_gain: float32 [2048], replicated, may hold values from 0.1 to 1.9
- w_in: float32 [2048, 512], P('fs', 'tp'), may hold values from -0.125 to 0.125
- s_in: float32 [512], P(('tp', 'fs')), may hold values from 0.1 to 1.9
- pool_w: bfloat16 [4, 128, 128], replicated, may hold values from -0.5 to 0.5
- w_out: float32 [512, 2048], P('fs', 'tp'), may hold values from -0.25 to 0.25
- s_out: float32 [2048], P(('tp', 'fs')), may hold values from 0.1 to 1.9
- ffn_gain: float32 [2048], replicated, may hold values from 0.1 to 1.9
- w_up: float32 [2048, 8192], P('fs', 'tp'), may hold values from -0.125 to 0.125
- s_up: float32 [8192], P(('tp', 'fs')), may hold values from 0.1 to 1.9
- w_down: float32 [8192, 2048], P('tp', 'fs'), may hold values from -0.0625 to 0.0625
- s_down: float32 [2048], P('fs'), may hold values from 0.1 to 1.9
Outputs:
- result: bfloat16 [32, 1024, 2048], P(('rep', 'fs'), None, 'tp')
All inputs are finite; a program needn't handle non-finite values.
Results may differ from a plain program's by a relative error of at most 0.012.
Values may be sent and summed in bfloat16 or wider, within the bound.
No kernel may reach another device: no remote copies, remote signals or barrier semaphores. Data moves between devices by JAX's collectives and lax.ppermute only.
A program may use at most 64 MiB of HBM per device.

v0:
```python
import jax
import jax.numpy as jnp
from jax import lax
from jax.sharding import Mesh
from jax.sharding import PartitionSpec as P

PW = 512
GROUP = 128
FS = ("fs_0", "fs_1")
REP_FS = ("rep", "fs_0", "fs_1")
TP_FS = ("tp", "fs_0", "fs_1")
epsilon = 0.25


def laid_out(parts, dim):
    parts = jnp.moveaxis(parts, 0, dim)
    lengths = parts.shape
    return parts.reshape(*lengths[:dim], lengths[dim] * lengths[dim + 1], *lengths[dim + 2 :])


def gather_packed(arrays, axis, dims):
    ravelled = jnp.concatenate([a.reshape(-1) for a in arrays])
    lines, at, finished = (lax.all_gather(ravelled, axis), 0, [])
    for a, dim in zip(arrays, dims):
        parts = lines[:, at : at + a.size].reshape(-1, *a.shape)
        finished.append(laid_out(parts, dim))
        at += a.size
    return tuple(finished)


def sent_to_all(array, axis):
    count = lax.axis_size(axis)
    return lax.all_to_all(
        jnp.broadcast_to(array[None], (count, *array.shape)), axis, 0, 0, tiled=True
    )


def collect(array, axis, dim):
    return laid_out(sent_to_all(array, axis), dim)


def stacked_from(array, axes, turns):
    parts = array
    for k in turns:
        parts = lax.all_gather(parts, axes[k])
    done = turns[::-1]
    back = [done.index(k) for k in range(len(axes))]
    parts = parts.transpose(*back, *range(len(axes), parts.ndim))
    return parts.reshape(-1, *array.shape)


def whole_of(array, axes, turns, dim):
    return laid_out(stacked_from(array, axes, turns), dim)


def cut_along(array, dim, count):
    lengths = array.shape
    parts = array.reshape(*lengths[:dim], count, lengths[dim] // count, *lengths[dim + 1 :])
    return jnp.moveaxis(parts, dim, 0)


def sent_and_summed(array, axis, dim):
    count = lax.axis_size(axis)
    parts = lax.all_to_all(cut_along(array, dim, count), axis, 0, 0, tiled=True)
    return jnp.sum(parts.astype(jnp.float32), axis=0)


def rms_rows(values, gain):
    floats = values.astype(jnp.float32)
    scale = lax.rsqrt(jnp.mean(floats * floats, axis=-1, keepdims=True) + epsilon)
    return (floats * scale * gain).astype(jnp.bfloat16)


def pool_local(pool_in, first):
    length, width = pool_in.shape
    positions = jnp.arange(length, dtype=jnp.int32)
    source = positions[None, :]
    target = positions[:, None]
    group_of = (first + jnp.arange(width, dtype=jnp.int32)) // GROUP
    means = jnp.zeros((length, width), jnp.float32)
    for level in range(4):
        half = 2**level
        band_ones = ((source >= target - half) & (source < target + half)).astype(jnp.bfloat16)
        counts = (jnp.minimum(positions + half, length) - jnp.maximum(positions - half, 0)).astype(
            jnp.float32
        )
        sums = jnp.dot(band_ones, pool_in, preferred_element_type=jnp.float32) / counts[:, None]
        means = jnp.where(group_of[None, :] == level, sums, means)
    return (means - pool_in.astype(jnp.float32)).astype(jnp.bfloat16)


def fold_rows(left, piece):
    return jnp.dot(left, piece, preferred_element_type=jnp.float32)


def on_device(
    stream, norm_gain, w_in, s_in, pool_w, w_out, s_out, ffn_gain, w_up, s_up, w_down, s_down
):
    tokens = stream[0]
    length = tokens.shape[0]
    scale_in, scale_out, scale_up, scale_down = gather_packed(
        (s_in, s_out, s_up, s_down), FS, (0, 0, 0, 0)
    )
    in_whole, out_whole = gather_packed(
        (w_in.astype(jnp.bfloat16), w_out.astype(jnp.bfloat16)), FS, (0, 0)
    )
    full_rows = lax.all_gather(tokens, "tp", axis=1, tiled=True)
    normed = rms_rows(full_rows, norm_gain)
    projected = jnp.dot(normed, in_whole, preferred_element_type=jnp.float32)
    pool_in = (projected * scale_in).astype(jnp.bfloat16)
    pooled = pool_local(pool_in, lax.axis_index("tp") * pool_in.shape[1])
    pooled_all = collect(pooled, "tp", 1)
    grouped = jnp.einsum(
        "lgc,gcd->lgd",
        pooled_all.reshape(length, 4, GROUP),
        pool_w,
        preferred_element_type=jnp.float32,
    )
    grouped = grouped.reshape(length, PW).astype(jnp.bfloat16)
    branch = jnp.dot(grouped, out_whole, preferred_element_type=jnp.float32)
    mixed = (tokens.astype(jnp.float32) + branch * scale_out).astype(jnp.bfloat16)
    mixed_full = lax.all_gather(mixed, "tp", axis=1, tiled=True)
    ffn_in = rms_rows(mixed_full, ffn_gain)
    upward = fold_rows(ffn_in, whole_of(w_up.astype(jnp.bfloat16), FS, (0, 1), 0))
    hidden = jnp.square(jax.nn.relu(upward * scale_up)).astype(jnp.bfloat16)
    partial_value = jnp.dot(
        hidden,
        whole_of(w_down.astype(jnp.bfloat16), FS, (0, 1), 1),
        preferred_element_type=jnp.float32,
    )
    rounded = lax.optimization_barrier((partial_value * scale_down).astype(jnp.bfloat16))
    summed = sent_and_summed(rounded.astype(jnp.float32).astype(jnp.bfloat16), "tp", 1)
    return (mixed.astype(jnp.float32) + summed).astype(jnp.bfloat16)[None]


def solution(mesh):
    finer = Mesh(
        mesh.devices.reshape(mesh.shape["rep"], 4, 4, mesh.shape["tp"]),
        ("rep", "fs_0", "fs_1", "tp"),
    )
    return jax.shard_map(
        on_device,
        mesh=finer,
        in_specs=(
            P(REP_FS, None, "tp"),
            P(),
            P(FS, "tp"),
            P(TP_FS),
            P(),
            P(FS, "tp"),
            P(TP_FS),
            P(),
            P(FS, "tp"),
            P(TP_FS),
            P("tp", FS),
            P(FS),
        ),
        out_specs=P(REP_FS, None, "tp"),
        check_vma=False,
    )
```

profile of v0, /device:TPU:1, one launch (start us, length us, event | category | flops | bytes accessed | tf_op | source)
XLA Modules:
  0.0 350.2 jit_solution(10267729505535979363)
XLA Ops:
  6.5 1.8 convert_element_type.116
  8.4 1.8 convert_element_type.118
  10.3 0.7 all-gather.16.cloned.1.call-update
  11.0 34.7 %all-gather.18.cloned.1.call-done = bf16[512,1024]{1,0:T(8,128)(2,1)} async-done(((bf16[128,1024]{1,0:T(8,128)(2,1)}), bf16[512,1024]{1,0:T(8,128)(2,1)}) %all-gather.18.cloned.1.call-update) | async-done | bytes 1048592 | tf_op jit(solution)/shard_map/all_gather | solution.py:45
  45.8 0.8 convert_element_type.100
  46.8 0.8 convert_bitcast_fusion
  47.6 1.3 dynamic-slice
  49.6 0.9 maximum_dynamic-update-slice_fusion
  50.5 64.0 %all-reduce = f32[3392]{0:T(1024)S(1)} all-reduce(f32[3392]{0:T(1024)S(1)} %maximum_dynamic-update-slice_fusion), channel_id=4, replica_groups=mesh['rep'=2,'fs_0'=4,'fs_1'=4,'tp'=8] {'fs_0','fs_1'}, use_global_device_ids=true, to_apply=%add | all-reduce | flops 3392 | bytes 27136
  114.7 33.1 %all-gather.1 = bf16[262144]{0:T(1024)(128)(2,1)S(1)} all-gather(bf16[16384]{0:T(1024)(128)(2,1)S(1)} %pad_maximum_fusion), channel_id=3, replica_groups=mesh['rep'=2,'fs_0'=4,'fs_1'=4,'tp'=8] {'fs_0','fs_1'}, dimensions={0}, use_global_device_ids=true | all-gather | bytes 557056 | tf_op jit(solution)/shard_map/all_gather | solution.py:23
  148.2 0.5 reshape_reshape.12
  148.9 3.3 fusion.3
  152.4 1.5 fusion.69
  153.9 1.4 fusion.63
  155.3 1.4 fusion.57
  156.7 1.4 fusion.51
  158.1 1.4 fusion.72
  159.5 1.1 broadcast_in_dim.54
  160.6 26.7 %all-to-all-start = ((bf16[8,1024,64]{1,2,0:T(8,128)(2,1)}), bf16[8,1024,64]{1,2,0:T(8,128)(2,1)S(1)}, u32[]{:S(2)}, u32[]{:S(2)}) async-start(bf16[8,1024,64]{1,2,0:T(8,128)(2,1)} %broadcast_in_dim.54), calls=%async_computation | async-start | bytes 2097152 | tf_op jit(solution)/shard_map/all_to_all | solution.py:33
  187.6 14.7 %all-to-all-done = bf16[8,1024,64]{1,2,0:T(8,128)(2,1)S(1)} async-done(((bf16[8,1024,64]{1,2,0:T(8,128)(2,1)}), bf16[8,1024,64]{1,2,0:T(8,128)(2,1)S(1)}, u32[]{:S(2)}, u32[]{:S(2)}) %all-to-all-start) | async-done | bytes 1048608 | tf_op jit(solution)/shard_map/all_to_all | solution.py:33
  202.8 1.3 fusion.38
  204.3 4.8 %copy.28 = bf16[4,4,128,1024]{3,2,1,0:T(8,128)(2,1)} copy(bf16[4,4,128,1024]{3,2,0,1:T(8,128)(2,1)} %bitcast.61) | data formatting | bytes 8388608 | tf_op jit(solution)/shard_map/transpose | solution.py:48
  209.1 18.8 %all-gather.24.cloned.1.call-done = bf16[16,1024,128]{2,1,0:T(8,128)(2,1)} async-done(((bf16[4,1024,128]{2,1,0:T(8,128)(2,1)}), bf16[16,1024,128]{2,1,0:T(8,128)(2,1)}) %all-gather.24.cloned.1.call-update) | async-done | bytes 4194320 | tf_op jit(solution)/shard_map/all_gather | solution.py:45
  227.9 4.5 %copy.29 = bf16[4,4,1024,128]{3,2,1,0:T(8,128)(2,1)} copy(bf16[4,4,1024,128]{3,2,0,1:T(8,128)(2,1)} %bitcast.62) | data formatting | bytes 8388608 | tf_op jit(solution)/shard_map/transpose | solution.py:48
  232.4 6.4 %copy.30 = bf16[1024,16,128]{0,2,1:T(8,128)(2,1)} copy(bf16[1024,16,128]{2,0,1:T(8,128)(2,1)} %bitcast.59) | data formatting | bytes 8388608 | tf_op jit(solution)/shard_map/transpose | solution.py:16
  238.8 29.7 %all-gather.14.cloned.1.call-done = bf16[1024,2048]{1,0:T(8,128)(2,1)} async-done(((bf16[1024,256]{1,0:T(8,128)(2,1)}), bf16[1024,2048]{1,0:T(8,128)(2,1)}) %all-gather.14.cloned.1.call-update) | async-done | bytes 4194320 | tf_op jit(solution)/shard_map/all_gather | solution.py:122
  268.6 3.1 fusion
  271.6 14.6 %multiply_convert_fusion = bf16[1024,2048]{1,0:T(8,128)(2,1)} fusion(bf16[1024,2048]{0,1:T(8,128)(2,1)} %bitcast.64, f32[2048]{0:T(1024)S(1)} %slice_bitcast_fusion, f32[1024]{0:T(1024)S(1)} %mul.98, bf16[2048,1024]{1,0:T(8,128)(2,1)} %bitcast.63, bf16[1024,2048]{1,0:T(8,128)(2,1)} %all-gather.14.cloned.1.call-done, f32[2048]{0:T(1024)S(1)} %copy-done.5, ...), kind=kOutput, calls=%fused_computation.11 | convolution fusion | flops 8606711808 | bytes 16801792 | tf_op jit(solution)/shard_map/dot_general | solution.py:126
  286.3 2.5 copy.37
  288.7 52.6 %all_to_all.10 = bf16[8,1024,256]{2,1,0:T(8,128)(2,1)S(1)} all-to-all(bf16[8,1024,256]{2,1,0:T(8,128)(2,1)S(1)} %bitcast.60), channel_id=1, replica_groups=mesh['rep'=2,'fs_0'=4,'fs_1'=4,'tp'=8] {'tp'}, dimensions={0} | all-to-all | bytes 8388608 | tf_op jit(solution)/shard_map/all_to_all | solution.py:64
  341.4 0.6 convert_reduce_fusion
  342.4 0.9 fusion.79
  (55 shorter events, 2.8 us)
Async XLA Ops:
  6.5 195.7 %copy-start = (bf16[4,128,128]{2,1,0:T(8,128)(2,1)S(1)}, bf16[4,128,128]{2,1,0:T(8,128)(2,1)}, u32[]{:S(2)}) copy-start(bf16[4,128,128]{2,1,0:T(8,128)(2,1)} %param.16) | copy-start | bytes 393220
  6.5 39.2 %all-gather.18.cloned.1.call-start = ((), (), s32[]{:S(2)}) async-start(), calls=%async_computation.4 | async-start | bytes 1310720 | tf_op jit(solution)/shard_map/all_gather | solution.py:45
  8.4 139.7 %all-gather.22.cloned.1.call-start = ((), (), s32[]{:S(2)}) async-start(), calls=%async_computation.6 | async-start | bytes 1310720 | tf_op jit(solution)/shard_map/all_gather | solution.py:45
  10.2 138.6 %all-gather.16.cloned.1.call-start = ((), (), s32[]{:S(2)}) async-start(), calls=%async_computation.3 | async-start | bytes 4718592 | tf_op jit(solution)/shard_map/all_gather | solution.py:107
  11.0 193.4 %all-gather.20.cloned.1.call-start = ((), (), s32[]{:S(2)}) async-start(), calls=%async_computation.5 | async-start | bytes 5242880 | tf_op jit(solution)/shard_map/all_gather | solution.py:45
  45.8 182.1 %all-gather.24.cloned.1.call-start = ((), (), s32[]{:S(2)}) async-start(), calls=%async_computation.7 | async-start | bytes 5242880 | tf_op jit(solution)/shard_map/all_gather | solution.py:45
  147.8 4.3 %copy-start.4 = (f32[2048]{0:T(1024)S(1)}, f32[2048]{0:T(1024)}, u32[]{:S(2)}) copy-start(f32[2048]{0:T(1024)} %param.13) | copy-start | bytes 24580
  148.9 3.5 %copy-start.1 = (bf16[1,1024,2048]{2,1,0:T(8,128)(2,1)S(1)}, bf16[1,1024,2048]{2,1,0:T(8,128)(2,1)}, u32[]{:S(2)}) copy-start(bf16[1,1024,2048]{2,1,0:T(8,128)(2,1)} %all-gather.16.cloned.1.call-done) | copy-start | bytes 12582916
  158.1 44.7 %copy-start.3 = (bf16[1,1024,256]{2,1,0:T(8,128)(2,1)S(1)}, bf16[1,1024,256]{2,1,0:T(8,128)(2,1)}, u32[]{:S(2)}) copy-start(bf16[1,1024,256]{2,1,0:T(8,128)(2,1)} %param.12) | copy-start | bytes 1572868
  160.6 41.7 %all-to-all-start = ((bf16[8,1024,64]{1,2,0:T(8,128)(2,1)}), bf16[8,1024,64]{1,2,0:T(8,128)(2,1)S(1)}, u32[]{:S(2)}, u32[]{:S(2)}) async-start(bf16[8,1024,64]{1,2,0:T(8,128)(2,1)} %broadcast_in_dim.54), calls=%async_computation | async-start | bytes 2097152 | tf_op jit(solution)/shard_map/all_to_all | solution.py:33
  187.3 81.3 %all-gather.14.cloned.1.call-start = ((), (), s32[]{:S(2)}) async-start(), calls=%async_computation.2 | async-start | bytes 4718592 | tf_op jit(solution)/shard_map/all_gather | solution.py:122
  238.8 32.8 %copy-start.5 = (f32[2048]{0:T(1024)S(1)}, f32[2048]{0:T(1024)}, u32[]{:S(2)}) copy-start(f32[2048]{0:T(1024)} %param.19) | copy-start | bytes 24580
  341.4 1.0 copy-start.2
Sparse Core Ops, SparseCore 0:
  9.1 36.5 all-gather.17
  47.5 33.1 all-gather.21
  82.6 37.5 all-gather.15
  121.8 54.8 all-gather.19
  178.4 49.4 all-gather.23
  229.6 38.9 all-gather.13
where the time goes:
time: 351 us; the launch traced here: 350 us
  blocking collectives  150 us (43%)
  waiting for transfers between devices  98.7 us (28%)
  starting transfers between devices  26.9 us (8%)
  matrix products  23.5 us (7%)
  local copies, waits for them, and re-layouts  23.1 us (7%)
  between operations  14.4 us (4%)
  other arithmetic  13.9 us (4%)
    unnamed x1, blocking collectives  64 us
    all_gather x4, waiting for transfers between devices, stacked_from(): parts = lax.all_gather(parts, axes[k])  53.5 us
    all_to_all x1, blocking collectives, sent_and_summed(): parts = lax.all_to_all(cut_along(array, dim, count), axis, 0, 0, tiled=True)  52.6 us
    all_gather x1, blocking collectives, gather_packed(): lines, at, finished = (lax.all_gather(ravelled, axis), 0, [])  33.1 us
    all_gather x1, waiting for transfers between devices, on_device(): mixed_full = lax.all_gather(mixed, 'tp', axis=1, tiled=True)  29.7 us
    all_to_all x1, starting transfers between devices, sent_to_all(): lax.all_to_all(jnp.broadcast_to(array[None], (count, *array.shape)), axis...  26.7 us
    all_to_all x1, waiting for transfers between devices, sent_to_all(): lax.all_to_all(jnp.broadcast_to(array[None], (count, *array.shape)), axis...  14.7 us
    dot_general x1, matrix products, on_device(): jnp.dot(hidden, whole_of(w_down.astype(jnp.bfloat16), FS, (0, 1), 1), pre...  14.6 us
  transfers between devices with their start and end apart: 7, of which 4 were waited for; matrix products, arithmetic and copies ran while one was open for 10% of the time, Pallas kernels for 0%

commit v1 on v0

--- a/solution.py
+++ b/solution.py
@@ -3,6 +3,7 @@
 from jax import lax
 from jax.sharding import Mesh
 from jax.sharding import PartitionSpec as P
+from jax.lax import axis_index, axis_size, ppermute
 
 PW = 512
 GROUP = 128
@@ -10,6 +11,26 @@
 REP_FS = ("rep", "fs_0", "fs_1")
 TP_FS = ("tp", "fs_0", "fs_1")
 epsilon = 0.25
+
+
+def watch_the_shards(sheet, in_dim):
+    wide_out = list(sheet.shape[1:])
+    wide_out[in_dim] *= sheet.shape[0]
+    return jnp.moveaxis(sheet, 0, in_dim).reshape(wide_out)
+
+
+def state_open(state, ax_name):
+    devs = axis_size(ax_name)
+    block_next = state[None]
+    for j0 in range(devs.bit_length() - 1):
+        known = 1 << j0
+        kept_arr = ppermute(
+            block_next, axis_name=ax_name, perm=tuple(((t, t ^ known) for t in range(devs)))
+        )
+        placed = jnp.stack([block_next, kept_arr])
+        z_new = axis_index(ax_name) >> j0 & 1
+        block_next = jnp.where(z_new == 0, placed, placed[::-1]).reshape(-1, *state.shape)
+    return block_next
 
 
 def laid_out(parts, dim):
@@ -119,7 +140,7 @@
     grouped = grouped.reshape(length, PW).astype(jnp.bfloat16)
     branch = jnp.dot(grouped, out_whole, preferred_element_type=jnp.float32)
     mixed = (tokens.astype(jnp.float32) + branch * scale_out).astype(jnp.bfloat16)
-    mixed_full = lax.all_gather(mixed, "tp", axis=1, tiled=True)
+    mixed_full = watch_the_shards(state_open(mixed, "tp"), 1)
     ffn_in = rms_rows(mixed_full, ffn_gain)
     upward = fold_rows(ffn_in, whole_of(w_up.astype(jnp.bfloat16), FS, (0, 1), 0))
     hidden = jnp.square(jax.nn.relu(upward * scale_up)).astype(jnp.bfloat16)

time: 351 us -> 369 us (1.051)
  waiting for transfers between devices: 98.7 us -> 106 us
  other arithmetic: 13.9 us -> 20 us
    ppermute x0 -> x3, waiting for transfers between devices: none -> 56.4 us  [state_open(): ppermute(block_next, axis_name=ax_name, perm=tuple(((t, t ^ known) for t...]
    all_gather x1 -> x0, waiting for transfers between devices: 29.7 us -> none  [on_device(): mixed_full = lax.all_gather(mixed, 'tp', axis=1, tiled=True)]
    all_gather x4, waiting for transfers between devices: 53.5 us -> 34.7 us  [stacked_from(): parts = lax.all_gather(parts, axes[k])]
    another operation x0 -> x4, other arithmetic: none -> 3.91 us  [state_open(): placed = jnp.stack([block_next, kept_arr])]
  transfers between devices with their start and end apart: 7 -> 9, of which waited for: 4 -> 5; matrix products, arithmetic and copies ran while one was open for 10% -> 11% of each run, Pallas kernels for 0% -> 0%
where the time goes in v1:
time: 369 us; the launch traced here: 368 us
  blocking collectives  151 us (41%)
  waiting for transfers between devices  106 us (29%)
  starting transfers between devices  29.4 us (8%)
  local copies, waits for them, and re-layouts  24.7 us (7%)
  matrix products  23.1 us (6%)
  other arithmetic  20 us (5%)
  between operations  14.1 us (4%)
    unnamed x1, blocking collectives  63.9 us
    ppermute x3, waiting for transfers between devices, state_open(): ppermute(block_next, axis_name=ax_name, perm=tuple(((t, t ^ known) for t...  56.4 us
    all_to_all x1, blocking collectives, sent_and_summed(): parts = lax.all_to_all(cut_along(array, dim, count), axis, 0, 0, tiled=True)  53.3 us
    all_gather x4, waiting for transfers between devices, stacked_from(): parts = lax.all_gather(parts, axes[k])  34.7 us
    all_gather x1, blocking collectives, gather_packed(): lines, at, finished = (lax.all_gather(ravelled, axis), 0, [])  33.7 us
    all_to_all x1, starting transfers between devices, sent_to_all(): lax.all_to_all(jnp.broadcast_to(array[None], (count, *array.shape)), axis...  26.7 us
    dot_general x1, matrix products, on_device(): jnp.dot(hidden, whole_of(w_down.astype(jnp.bfloat16), FS, (0, 1), 1), pre...  14.4 us
    all_to_all x1, waiting for transfers between devices, sent_to_all(): lax.all_to_all(jnp.broadcast_to(array[None], (count, *array.shape)), axis...  13.9 us
  transfers between devices with their start and end apart: 9, of which 5 were waited for; matrix products, arithmetic and copies ran while one was open for 11% of the time, Pallas kernels for 0%

profile of v1, /device:TPU:1, one launch (start us, length us, event | category | flops | bytes accessed | tf_op | source)
XLA Modules:
  0.0 368.2 jit_solution(15633538210918152489)
XLA Ops:
  6.5 1.8 convert_element_type.133
  8.4 1.8 convert_element_type.131
  11.0 34.7 %all-gather.19.cloned.1.call-done = bf16[4096,128]{1,0:T(8,128)(2,1)} async-done(((bf16[1024,128]{1,0:T(8,128)(2,1)}), bf16[4096,128]{1,0:T(8,128)(2,1)}) %all-gather.19.cloned.1.call-update) | async-done | bytes 1048592 | tf_op jit(solution)/shard_map/all_gather | solution.py:66
  45.8 1.3 dynamic-slice
  48.7 63.9 %all-reduce = f32[3392]{0:T(1024)S(1)} all-reduce(f32[3392]{0:T(1024)S(1)} %maximum_dynamic-update-slice_fusion), channel_id=4, replica_groups=mesh['rep'=2,'fs_0'=4,'fs_1'=4,'tp'=8] {'fs_0','fs_1'}, use_global_device_ids=true, to_apply=%add | all-reduce | flops 3392 | bytes 27136
  114.6 33.7 %all-gather.1 = bf16[262144]{0:T(1024)(128)(2,1)S(1)} all-gather(bf16[16384]{0:T(1024)(128)(2,1)S(1)} %pad_maximum_fusion.3), channel_id=3, replica_groups=mesh['rep'=2,'fs_0'=4,'fs_1'=4,'tp'=8] {'fs_0','fs_1'}, dimensions={0}, use_global_device_ids=true | all-gather | bytes 557056 | tf_op jit(solution)/shard_map/all_gather | solution.py:44
  149.3 3.3 fusion
  152.9 1.5 fusion.63
  154.3 1.4 fusion.57
  155.7 1.4 fusion.51
  157.1 1.4 fusion.45
  158.5 1.4 fusion.66
  159.9 1.2 broadcast_in_dim.57
  161.1 26.7 %all-to-all-start = ((bf16[8,1024,64]{1,2,0:T(8,128)(2,1)}), bf16[8,1024,64]{1,2,0:T(8,128)(2,1)S(1)}, u32[]{:S(2)}, u32[]{:S(2)}) async-start(bf16[8,1024,64]{1,2,0:T(8,128)(2,1)} %broadcast_in_dim.57), calls=%async_computation | async-start | bytes 2097152 | tf_op jit(solution)/shard_map/all_to_all | solution.py:54
  188.9 13.9 %all-to-all-done = bf16[8,1024,64]{1,2,0:T(8,128)(2,1)S(1)} async-done(((bf16[8,1024,64]{1,2,0:T(8,128)(2,1)}), bf16[8,1024,64]{1,2,0:T(8,128)(2,1)S(1)}, u32[]{:S(2)}, u32[]{:S(2)}) %all-to-all-start) | async-done | bytes 1048608 | tf_op jit(solution)/shard_map/all_to_all | solution.py:54
  203.3 1.2 fusion.32
  204.5 1.1 collective-permute-start
  205.5 1.5 collective-permute-done
  208.1 24.2 %collective-permute-done.1 = bf16[2,1024,256]{1,2,0:T(8,128)(2,1)} collective-permute-done((bf16[2,1024,256]{1,2,0:T(8,128)(2,1)S(1)}, bf16[2,1024,256]{1,2,0:T(8,128)(2,1)}, u32[]{:S(2)}, u32[]{:S(2)}) %collective-permute-start.1) | collective-permute-done | bytes 1048608 | tf_op jit(solution)/shard_map/ppermute | solution.py:27
  232.3 1.4 pad_maximum_fusion.1
  235.5 4.6 %copy.36 = bf16[4,4,1024,128]{3,2,1,0:T(8,128)(2,1)} copy(bf16[4,4,1024,128]{3,2,0,1:T(8,128)(2,1)} %bitcast.82) | data formatting | bytes 8388608 | tf_op jit(solution)/shard_map/transpose | solution.py:69
  240.1 6.5 %copy.37 = bf16[1024,16,128]{0,2,1:T(8,128)(2,1)} copy(bf16[1024,16,128]{2,0,1:T(8,128)(2,1)} %bitcast.78) | data formatting | bytes 8388608 | tf_op jit(solution)/shard_map/transpose | solution.py:37
  246.5 4.8 %copy.35 = bf16[4,4,128,1024]{3,2,1,0:T(8,128)(2,1)} copy(bf16[4,4,128,1024]{3,2,0,1:T(8,128)(2,1)} %bitcast.83) | data formatting | bytes 8388608 | tf_op jit(solution)/shard_map/transpose | solution.py:69
  251.3 30.7 %collective-permute-done.2 = bf16[4,1024,256]{1,2,0:T(8,128)(2,1)} collective-permute-done((bf16[4,1024,256]{1,2,0:T(8,128)(2,1)S(1)}, bf16[4,1024,256]{1,2,0:T(8,128)(2,1)}, u32[]{:S(2)}, u32[]{:S(2)}) %collective-permute-start.2) | collective-permute-done | bytes 2097184 | tf_op jit(solution)/shard_map/ppermute | solution.py:27
  282.0 2.0 pad_maximum_fusion
  283.9 1.4 reverse_select_fusion
  285.4 1.2 fusion.3
  286.6 2.8 fusion.5
  289.4 14.4 %multiply_convert_fusion = bf16[1024,2048]{1,0:T(8,128)(2,1)} fusion(bf16[1024,2048]{0,1:T(8,128)(2,1)} %bitcast.84, f32[2048]{0:T(1024)S(1)} %slice_bitcast_fusion, bf16[1024,2048]{0,1:T(8,128)(2,1)} %bitcast.86, bf16[2048,1024]{1,0:T(8,128)(2,1)} %bitcast.85, f32[1024]{0:T(1024)S(1)} %mul.107), kind=kOutput, calls=%fused_computation.11 | convolution fusion | flops 8598323200 | bytes 16789504 | tf_op jit(solution)/shard_map/dot_general | solution.py:147
  303.8 2.5 copy.48
  306.2 53.3 %all_to_all.10 = bf16[8,1024,256]{2,1,0:T(8,128)(2,1)S(1)} all-to-all(bf16[8,1024,256]{2,1,0:T(8,128)(2,1)S(1)} %bitcast.79), channel_id=1, replica_groups=mesh['rep'=2,'fs_0'=4,'fs_1'=4,'tp'=8] {'tp'}, dimensions={0} | all-to-all | bytes 8388608 | tf_op jit(solution)/shard_map/all_to_all | solution.py:85
  360.6 1.0 copy.41
  (69 shorter events, 10.3 us)
Async XLA Ops:
  6.5 196.3 %copy-start = (bf16[4,128,128]{2,1,0:T(8,128)(2,1)S(1)}, bf16[4,128,128]{2,1,0:T(8,128)(2,1)}, u32[]{:S(2)}) copy-start(bf16[4,128,128]{2,1,0:T(8,128)(2,1)} %param.16) | copy-start | bytes 393220
  6.5 39.2 %all-gather.19.cloned.1.call-start = ((), (), s32[]{:S(2)}) async-start(), calls=%async_computation.5 | async-start | bytes 1310720 | tf_op jit(solution)/shard_map/all_gather | solution.py:66
  8.4 140.9 %all-gather.15.cloned.1.call-start = ((), (), s32[]{:S(2)}) async-start(), calls=%async_computation.3 | async-start | bytes 1310720 | tf_op jit(solution)/shard_map/all_gather | solution.py:66
  10.3 139.1 %all-gather.13.cloned.1.call-start = ((), (), s32[]{:S(2)}) async-start(), calls=%async_computation.2 | async-start | bytes 4718592 | tf_op jit(solution)/shard_map/all_gather | solution.py:128
  11.0 224.5 %all-gather.21.cloned.1.call-start = ((), (), s32[]{:S(2)}) async-start(), calls=%async_computation.6 | async-start | bytes 5242880 | tf_op jit(solution)/shard_map/all_gather | solution.py:66
  45.8 200.8 %all-gather.17.cloned.1.call-start = ((), (), s32[]{:S(2)}) async-start(), calls=%async_computation.4 | async-start | bytes 5242880 | tf_op jit(solution)/shard_map/all_gather | solution.py:66
  148.3 4.4 %copy-start.5 = (f32[2048]{0:T(1024)S(1)}, f32[2048]{0:T(1024)}, u32[]{:S(2)}) copy-start(f32[2048]{0:T(1024)} %param.13) | copy-start | bytes 24580
  149.3 3.5 copy-start.2
  158.5 29.4 %copy-start.3 = (bf16[1,1024,256]{2,1,0:T(8,128)(2,1)S(1)}, bf16[1,1024,256]{2,1,0:T(8,128)(2,1)}, u32[]{:S(2)}) copy-start(bf16[1,1024,256]{2,1,0:T(8,128)(2,1)} %param.12) | copy-start | bytes 1572868
  161.1 41.7 %all-to-all-start = ((bf16[8,1024,64]{1,2,0:T(8,128)(2,1)}), bf16[8,1024,64]{1,2,0:T(8,128)(2,1)S(1)}, u32[]{:S(2)}, u32[]{:S(2)}) async-start(bf16[8,1024,64]{1,2,0:T(8,128)(2,1)} %broadcast_in_dim.57), calls=%async_computation | async-start | bytes 2097152 | tf_op jit(solution)/shard_map/all_to_all | solution.py:54
  204.5 2.6 collective-permute-start
  207.6 24.7 %collective-permute-start.1 = (bf16[2,1024,256]{1,2,0:T(8,128)(2,1)S(1)}, bf16[2,1024,256]{1,2,0:T(8,128)(2,1)}, u32[]{:S(2)}, u32[]{:S(2)}) collective-permute-start(bf16[2,1024,256]{1,2,0:T(8,128)(2,1)S(1)} %get-tuple-element.6), channel_id=1, source_target_pairs={{0,2},{1,3},{2,0},{3,1},{4,6},{5,7},{6,4},{7,5},{8,10},{9,11},{10,... | collective-permute-start | bytes 3145736 | tf_op jit(solution)/shard_map/ppermute | solution.py:27
  232.3 3.1 copy-start.4
  234.3 47.7 %collective-permute-start.2 = (bf16[4,1024,256]{1,2,0:T(8,128)(2,1)S(1)}, bf16[4,1024,256]{1,2,0:T(8,128)(2,1)}, u32[]{:S(2)}, u32[]{:S(2)}) collective-permute-start(bf16[4,1024,256]{1,2,0:T(8,128)(2,1)S(1)} %bitcast.80), channel_id=1, source_target_pairs={{0,4},{1,5},{2,6},{3,7},{4,0},{5,1},{6,2},{7,3},{8,12},{9,13},{10,... | collective-permute-start | bytes 6291464 | tf_op jit(solution)/shard_map/ppermute | solution.py:27
  306.2 55.4 %copy-start.1 = (bf16[4,128,128]{2,1,0:T(8,128)(2,1)S(1)}, bf16[4,128,128]{2,1,0:T(8,128)(2,1)}, u32[]{:S(2)}) copy-start(bf16[4,128,128]{2,1,0:T(8,128)(2,1)} %param.16) | copy-start | bytes 393220
Sparse Core Ops, SparseCore 0:
  9.1 36.5 all-gather.18
  47.5 33.1 all-gather.14
  82.6 37.4 all-gather.12
  121.8 54.6 all-gather.20
  178.2 49.5 all-gather.16
